TPU v7x, 32 devices: a whole 2x2x4 slice. The times are simulated.
32 devices in a mesh: ep: 8 (over z, y), tp: 4 (over x, core).
Axes of the slice: x: 2, y: 2, z: 4, core: 2. Of those that a mesh axis runs over, the one named last changes fastest.
Arguments:
- queries_a: bfloat16 [1024, 1024], P('ep', 'tp'), may hold values from -128 to 128
- queries_b: bfloat16 [1024, 1024], P('ep', 'tp'), may hold values from -128 to 128
- keys_a: bfloat16 [1024, 512], P('ep', 'tp'), may hold values from -8 to 8
- keys_b: bfloat16 [1024, 512], P('ep', 'tp'), may hold values from -8 to 8
- values: bfloat16 [1024, 1024], P('ep', 'tp'), may hold values from -6 to 6
- lambdas: float32 [16], P('tp'), may hold values from 0.3 to 0.8
- head_gain: float32 [128], replicated, may hold values from 0.1 to 1.9
- w_out: bfloat16 [2048, 2048], P('tp'), may hold values from -0.125 to 0.125
- moe_tokens: bfloat16 [4096, 2048], P(('ep', 'tp')), may hold values from -80 to 80
- moe_gain: float32 [2048], replicated, may hold values from 0.1 to 1.9
- routes: int32 [4096, 2], P(('ep', 'tp')), may hold values from 0 to 7, all different within a row; in each aligned block of 128 rows (0 to 127, 128 to 255, ...) at most 48 rows name the same one
- route_weights: float32 [4096, 2], P(('ep', 'tp')), may hold values from 0.1 to 1
- w_gate: bfloat16 [8, 2048, 2048], P('ep', None, 'tp'), may hold values from -4 to 4
- w_up: bfloat16 [8, 2048, 2048], P('ep', None, 'tp'), may hold values from -4 to 4
- w_down: bfloat16 [8, 2048, 2048], P('ep', 'tp'), may hold values from -0.0625 to 0.0625
Outputs:
- mixer_out: bfloat16 [1024, 2048], P(('ep', 'tp'))
- moe_out: bfloat16 [4096, 2048], P(('ep', 'tp'))
Inputs may be any that keep to these rules, and one draw needn't show every extreme that they name: `routes`: each row names 2 different experts. Within the rows of one device no expert is named by more than 48 rows, a bound that some block reaches of some device.
All inputs are finite; a program needn't handle non-finite values.
Results may differ from a plain program's by a relative error of at most 0.011.
Values may be sent and summed in bfloat16 or wider, within the bound.
A program may use at most 192 MiB of HBM per device.

v0:
```python
import jax
import jax.numpy as jnp
from jax import lax
from jax.sharding import PartitionSpec as P

HEAD = 64
VDIM = 128
TOP = 2
eps = 1e-05
alpha_act = 1.702
limit_act = 7.0
negative = -1e30


def clamped_unit(gate, up):
    capped = jnp.minimum(gate, limit_act)
    linear = jnp.clip(up, -limit_act, limit_act)
    return capped * jax.nn.sigmoid(alpha_act * capped) * (linear + 1.0)


def hidden_rows(inputs, gate_matrix, up_matrix):
    gate = jnp.dot(inputs, gate_matrix, preferred_element_type=jnp.float32)
    up = jnp.dot(inputs, up_matrix, preferred_element_type=jnp.float32)
    return clamped_unit(gate, up).astype(jnp.bfloat16)


def pick_rows(table, owner):
    valid = owner < table.shape[0]
    chosen = jnp.take(table, jnp.minimum(owner, table.shape[0] - 1), axis=0)
    return jnp.where(valid[:, None], chosen, jnp.zeros_like(chosen))


def mixer(queries_a, queries_b, keys_a, keys_b, values, lambdas, head_gain, w_out):
    tokens = queries_a.shape[0]
    local_heads = lambdas.shape[0]
    kv_local = keys_a.shape[1] // HEAD
    group = local_heads // kv_local
    scale = HEAD ** (-0.5)
    query_pos = lax.axis_index("ep") * tokens + jnp.arange(tokens, dtype=jnp.int32)
    grouped_a = queries_a.reshape(tokens, kv_local, group, HEAD)
    grouped_b = queries_b.reshape(tokens, kv_local, group, HEAD)
    lowest = jnp.full((kv_local, group, tokens), negative, jnp.float32)
    nothing = jnp.zeros((kv_local, group, tokens), jnp.float32)
    blank = jnp.zeros((kv_local, group, tokens, VDIM), jnp.float32)

    def one_map(grouped, keys, value_rows, visible, state):
        peak, total, accum = state
        scores = (
            jnp.einsum("rgjd,ngd->gjrn", grouped, keys, preferred_element_type=jnp.float32) * scale
        )
        scores = jnp.where(visible, scores, negative)
        new_peak = jnp.maximum(peak, jnp.max(scores, axis=-1))
        expo = jnp.where(visible, jnp.exp(scores - new_peak[..., None]), 0.0)
        total = jnp.sum(expo, axis=-1)
        accum = jnp.einsum(
            "gjrn,ngv->gjrv",
            expo.astype(jnp.bfloat16),
            value_rows,
            preferred_element_type=jnp.float32,
        )
        return (new_peak, total, accum)

    initial = (lowest, nothing, blank, lowest, nothing, blank)
    piece_a = lax.all_gather(keys_a, "ep", axis=0, tiled=True)
    piece_b = lax.all_gather(keys_b, "ep", axis=0, tiled=True)
    piece_v = lax.all_gather(values, "ep", axis=0, tiled=True)
    count = piece_a.shape[0]

    def visit(state):
        key_pos = jnp.arange(count, dtype=jnp.int32)
        visible = key_pos[None, :] <= query_pos[:, None]
        value_rows = piece_v.reshape(count, kv_local, VDIM)
        first = one_map(
            grouped_a, piece_a.reshape(count, kv_local, HEAD), value_rows, visible, state[:3]
        )
        second = one_map(
            grouped_b, piece_b.reshape(count, kv_local, HEAD), value_rows, visible, state[3:]
        )
        return first + second

    result = lax.cond(jnp.int32(0) <= query_pos[tokens - 1], visit, lambda state: state, initial)
    mixed_a = result[2] / result[1][..., None]
    mixed_b = result[5] / result[4][..., None]
    diff = mixed_a - lambdas.reshape(kv_local, group, 1, 1) * mixed_b
    heads_out = (
        diff * lax.rsqrt(jnp.mean(diff * diff, axis=-1, keepdims=True) + eps) * head_gain
    ).astype(jnp.bfloat16)
    weights_out = w_out.reshape(kv_local, group, VDIM, w_out.shape[1])
    return lax.psum_scatter(
        jnp.einsum(
            "gjrv,gjvd->rd", heads_out, weights_out, preferred_element_type=jnp.float32
        ).astype(jnp.bfloat16),
        "tp",
        scatter_dimension=0,
        tiled=True,
    )


def experts(moe_tokens, moe_gain, routes, route_weights, w_gate, w_up, w_down):
    tok_rows, width = moe_tokens.shape
    n_experts = lax.axis_size("ep") * w_gate.shape[0]
    capacity = max(2, 3 * tok_rows * TOP // (2 * n_experts))
    inputs = moe_tokens.astype(jnp.float32)
    normed = (
        inputs * lax.rsqrt(jnp.mean(inputs * inputs, axis=-1, keepdims=True) + eps) * moe_gain
    ).astype(jnp.bfloat16)
    chosen = routes.reshape(-1)
    member = (chosen[:, None] == jnp.arange(n_experts, dtype=jnp.int32)[None, :]).astype(jnp.int32)
    order_in = jnp.sum(jnp.cumsum(member, axis=0) * member, axis=1) - 1
    slot_ids = chosen * capacity + order_in
    owner = (
        jnp.full((n_experts * capacity,), tok_rows, jnp.int32)
        .at[slot_ids]
        .set(jnp.arange(tok_rows * TOP, dtype=jnp.int32) // TOP)
    )
    outgoing = pick_rows(normed, owner).reshape(n_experts, capacity, width)
    arrived = lax.all_to_all(outgoing, "ep", split_axis=0, concat_axis=1, tiled=True).reshape(
        -1, width
    )
    hidden = hidden_rows(lax.all_gather(arrived, "tp", axis=0, tiled=True), w_gate[0], w_up[0])
    expert_out = lax.psum_scatter(
        jnp.dot(hidden, w_down[0], preferred_element_type=jnp.float32).astype(jnp.bfloat16),
        "tp",
        scatter_dimension=0,
        tiled=True,
    )
    returned = lax.all_to_all(
        expert_out.reshape(-1, capacity, width), "ep", split_axis=0, concat_axis=0, tiled=True
    )
    picked = jnp.take(returned.reshape(-1, width), slot_ids, axis=0).reshape(tok_rows, TOP, width)
    return jnp.sum(picked.astype(jnp.float32) * route_weights[:, :, None], axis=1).astype(
        jnp.bfloat16
    )


def body(
    queries_a,
    queries_b,
    keys_a,
    keys_b,
    values,
    lambdas,
    head_gain,
    w_out,
    moe_tokens,
    moe_gain,
    routes,
    route_weights,
    w_gate,
    w_up,
    w_down,
):
    mixer_out = mixer(queries_a, queries_b, keys_a, keys_b, values, lambdas, head_gain, w_out)
    moe_out = experts(moe_tokens, moe_gain, routes, route_weights, w_gate, w_up, w_down)
    return (mixer_out, moe_out)


def solution(mesh):
    return jax.shard_map(
        body,
        mesh=mesh,
        in_specs=(
            P("ep", "tp"),
            P("ep", "tp"),
            P("ep", "tp"),
            P("ep", "tp"),
            P("ep", "tp"),
            P("tp"),
            P(),
            P("tp", None),
            P(("ep", "tp"), None),
            P(),
            P(("ep", "tp"), None),
            P(("ep", "tp"), None),
            P("ep", None, "tp"),
            P("ep", None, "tp"),
            P("ep", "tp", None),
        ),
        out_specs=(P(("ep", "tp"), None), P(("ep", "tp"), None)),
        check_vma=False,
    )
```

profile of v0, /device:TPU:0, one launch (start us, length us, event | category | flops | bytes accessed | tf_op | source)
XLA Modules:
  0.0 350.4 jit_solution(3916929698931288925)
XLA Ops:
  7.2 0.0 copy-start
  7.2 0.0 all-gather.2.cloned.1.call-start
  7.2 0.9 copy.49
  8.2 0.1 eq.26
  8.3 0.1 reshape.159
  8.4 0.7 broadcast_multiply_fusion
  9.1 0.6 reduce-window.6
  9.7 0.2 slice_reduce_fusion
  10.0 0.1 fusion.34
  10.1 0.1 copy.53
  10.2 0.1 mul.117
  10.3 1.4 scatter_custom_fusion
  11.8 0.1 broadcast_in_dim.77
  11.9 0.1 broadcast_in_dim.79
  12.0 1.2 fusion.27
  13.2 1.2 fusion.29
  14.5 3.1 gather_fusion
  17.6 1.7 select_select_fusion
  19.3 44.2 %all_to_all.14 = bf16[8,48,2048]{2,1,0:T(8,128)(2,1)} all-to-all(bf16[8,48,2048]{2,1,0:T(8,128)(2,1)S(1)} %select_select_fusion), channel_id=1, replica_groups=mesh['ep'=8,'tp'=4] {'ep'}, dimensions={0} | all-to-all | bytes 3145728 | tf_op jit(solution)/shard_map/all_to_all | solution.py:117
  63.5 0.0 all-gather.2.cloned.1.call-update
  63.5 0.0 reduce-scatter.5.cloned.1.call-start
  63.5 45.5 %all-gather.2.cloned.1.call-done = bf16[1536,2048]{1,0:T(8,128)(2,1)} async-done(((bf16[384,2048]{1,0:T(8,128)(2,1)}), bf16[1536,2048]{1,0:T(8,128)(2,1)}) %all-gather.2.cloned.1.call-update) | async-done | bytes 6291472 | tf_op jit(solution)/shard_map/all_gather | solution.py:120
  109.0 8.5 %convolution_minimum_fusion = f32[1536,512]{1,0:T(8,128)} fusion(bf16[1536,2048]{1,0:T(8,128)(2,1)} %all-gather.2.cloned.1.call-done, bf16[1,2048,512]{2,1,0:T(8,128)(2,1)} %param.29), kind=kOutput, calls=%fused_computation.30 | convolution fusion | flops 3222011904 | bytes 11534336 | tf_op jit(solution)/shard_map/dot_general | solution.py:22
  117.5 11.9 %convolution_convert_fusion = bf16[1536,2048]{1,0:T(8,128)(2,1)} fusion(bf16[1,512,2048]{2,1,0:T(8,128)(2,1)S(1)} %copy-done, bf16[1536,2048]{1,0:T(8,128)(2,1)} %all-gather.2.cloned.1.call-done, f32[1536,512]{1,0:T(8,128)} %convolution_minimum_fusion, bf16[1,2048,512]{2,1,0:T(8,128)(2,1)} %param.30), kind=kOutput, calls=%fused_computation.28 | convolution fusion | flops 6452674560 | bytes 19922944 | tf_op jit(solution)/shard_map/dot_general | solution.py:122
  129.4 0.0 reduce-scatter.5.cloned.1.call-update
  129.4 0.0 copy-start.8
  129.4 0.0 copy-start.9
  129.5 0.0 copy-start.15
  129.5 0.0 copy-start.6
  129.5 58.9 %reduce-scatter.5.cloned.1.call-done = bf16[384,2048]{1,0:T(8,128)(2,1)} async-done(((bf16[1536,2048]{1,0:T(8,128)(2,1)}), bf16[384,2048]{1,0:T(8,128)(2,1)}) %reduce-scatter.5.cloned.1.call-update) | async-done | bytes 1572880 | tf_op jit(solution)/shard_map/reduce_scatter | solution.py:121
  188.4 5.5 %all-to-all-start.1 = ((bf16[8,48,2048]{2,1,0:T(8,128)(2,1)}), bf16[8,48,2048]{2,1,0:T(8,128)(2,1)}, u32[]{:S(2)}, u32[]{:S(2)}) async-start(bf16[8,48,2048]{2,1,0:T(8,128)(2,1)} %bitcast.77), calls=%async_computation.3 | async-start | bytes 3145728 | tf_op jit(solution)/shard_map/all_to_all | solution.py:127
  193.9 0.0 reduce-scatter.3.cloned.1.call-start
  194.0 0.1 copy.45
  194.1 0.1 copy.46
  194.3 0.6 slice.9
  195.5 0.7 mul.106
  196.2 54.2 %all_gather.12 = bf16[1024,128]{0,1:T(8,128)(2,1)S(1)} all-gather(bf16[128,128]{0,1:T(8,128)(2,1)S(1)} %copy.45), channel_id=1, replica_groups=mesh['ep'=8,'tp'=4] {'ep'}, dimensions={0}, use_global_device_ids=true | all-gather | bytes 294912 | tf_op jit(solution)/shard_map/all_gather | solution.py:64
  250.3 27.8 %all_gather.14 = bf16[1024,128]{0,1:T(8,128)(2,1)} all-gather(bf16[128,128]{0,1:T(8,128)(2,1)S(1)} %copy.46), channel_id=1, replica_groups=mesh['ep'=8,'tp'=4] {'ep'}, dimensions={0}, use_global_device_ids=true | all-gather | bytes 294912 | tf_op jit(solution)/shard_map/all_gather | solution.py:65
  278.2 31.3 %all_gather.13 = bf16[1024,256]{1,0:T(8,128)(2,1)S(1)} all-gather(bf16[128,256]{1,0:T(8,128)(2,1)S(1)} %copy-done.6), channel_id=1, replica_groups=mesh['ep'=8,'tp'=4] {'ep'}, dimensions={0}, use_global_device_ids=true | all-gather | bytes 589824 | tf_op jit(solution)/shard_map/all_gather | solution.py:66
  309.5 12.2 %conditional.1 = (f32[2,2,128]{2,1,0:T(2,128)S(1)}, f32[2,2,128,128]{3,2,1,0:T(8,128)S(1)}, f32[2,2,128]{2,1,0:T(2,128)S(1)}, f32[2,2,128,128]{3,2,1,0:T(8,128)S(1)}) conditional(s32[]{:T(128)} %bitcast.12, () %tuple.16, (s32[128]{0:T(128)S(1)}, bf16[1024,128]{0,1:T(8,128)(2,1)S(1)}, bf16[128,256]{1,0:T(8,128)(2,1)}, bf16[1024,256]{1,0:T(8,128)(2,1)S(1)}, ...), branch_computations={%region_0.0_spmd, %region_1.6_spmd} | conditional | flops 416414720 | bytes 47481572 | solution.py:81
  309.5 0.1 iota_compare_fusion
  309.6 1.0 copy.47
  310.6 1.8 fusion.42
  312.4 0.1 copy.48
  312.5 2.4 fusion.1
  315.0 1.0 fusion.5
  316.0 0.2 copy-done.3
  316.3 0.1 reshape.149
  316.4 0.0 copy-start.5
  316.4 0.8 copy-done.5
  317.2 2.6 fusion.6
  319.8 1.9 fusion.8
  321.7 0.0 copy-start.14
  321.7 1.0 multiply_reduce_fusion.1
  322.7 2.9 fusion.23
  325.7 0.0 reduce-scatter.3.cloned.1.call-update
  325.7 0.1 sub.35
  325.8 0.1 copy.51
  325.9 0.1 copy.52
  326.1 0.1 copy.54
  326.2 4.0 %gather_fusion.1 = bf16[256,2048]{1,0:T(8,128)(2,1)S(1)} fusion(bf16[384,2048]{1,0:T(8,128)(2,1)} %bitcast.26, s32[1024]{0:T(1024)S(1)} %pad_clamp_fusion), kind=kCustom, calls=%fused_computation.1 | custom fusion | bytes 2098176 | tf_op jit(solution)/shard_map/jit(_take)/gather | solution.py:130
  330.2 1.5 gather.15
  331.7 6.2 %multiply_reduce_fusion = bf16[128,2048]{1,0:T(8,128)(2,1)} fusion(bf16[128,2,2048]{2,1,0:T(2,128)(2,1)} %gather.15, pred[128,2]{1,0:T(8,128)(4,1)S(1)} %copy.52, f32[128,2]{1,0:T(8,128)S(1)} %copy.54), kind=kLoop, calls=%fused_computation.39 | loop fusion | flops 1835008 | bytes 1574144 | tf_op jit(solution)/shard_map/reduce_sum | solution.py:131
  338.0 5.9 %reduce-scatter.3.cloned.1.call-done = bf16[32,2048]{1,0:T(8,128)(2,1)} async-done(((bf16[128,2048]{1,0:T(8,128)(2,1)}), bf16[32,2048]{1,0:T(8,128)(2,1)}) %reduce-scatter.3.cloned.1.call-update) | async-done | bytes 131088 | tf_op jit(solution)/shard_map/reduce_scatter | solution.py:89
  (39 shorter events, 0.2 us)
Async XLA Ops:
  7.2 110.4 %copy-start = (bf16[1,512,2048]{2,1,0:T(8,128)(2,1)S(1)}, bf16[1,512,2048]{2,1,0:T(8,128)(2,1)}, u32[]{:S(2)}) copy-start(bf16[1,512,2048]{2,1,0:T(8,128)(2,1)} %param.31) | copy-start | bytes 6291460
  7.2 101.8 %all-gather.2.cloned.1.call-start = ((), (), s32[]{:S(2)}) async-start(), calls=%async_computation.5 | async-start | bytes 7864320 | tf_op jit(solution)/shard_map/all_gather | solution.py:120
  10.3 1.4 copy-start.12
  63.5 124.9 %reduce-scatter.5.cloned.1.call-start = ((), (), s32[]{:S(2)}) async-start(), calls=%async_computation.6 | async-start | bytes 7864320 | tf_op jit(solution)/shard_map/reduce_scatter | solution.py:121
  129.4 64.6 %copy-start.8 = (bf16[128,128]{1,0:T(8,128)(2,1)S(1)}, bf16[128,128]{1,0:T(8,128)(2,1)}, u32[]{:S(2)}) copy-start(bf16[128,128]{1,0:T(8,128)(2,1)} %param.19) | copy-start | bytes 98308
  129.4 64.7 %copy-start.9 = (bf16[128,128]{1,0:T(8,128)(2,1)S(1)}, bf16[128,128]{1,0:T(8,128)(2,1)}, u32[]{:S(2)}) copy-start(bf16[128,128]{1,0:T(8,128)(2,1)} %param.20) | copy-start | bytes 98308
  129.5 66.0 %copy-start.15 = (f32[4]{0:T(128)S(1)}, f32[4]{0:T(128)}, u32[]{:S(2)}) copy-start(f32[4]{0:T(128)} %param.22) | copy-start | bytes 52
  129.5 148.7 %copy-start.6 = (bf16[128,256]{1,0:T(8,128)(2,1)S(1)}, bf16[128,256]{1,0:T(8,128)(2,1)}, u32[]{:S(2)}) copy-start(bf16[128,256]{1,0:T(8,128)(2,1)} %param.21) | copy-start | bytes 196612
  188.4 137.8 %all-to-all-start.1 = ((bf16[8,48,2048]{2,1,0:T(8,128)(2,1)}), bf16[8,48,2048]{2,1,0:T(8,128)(2,1)}, u32[]{:S(2)}, u32[]{:S(2)}) async-start(bf16[8,48,2048]{2,1,0:T(8,128)(2,1)} %bitcast.77), calls=%async_computation.3 | async-start | bytes 3145728 | tf_op jit(solution)/shard_map/all_to_all | solution.py:127
  193.9 149.9 %reduce-scatter.3.cloned.1.call-start = ((), (), s32[]{:S(2)}) async-start(), calls=%async_computation.4 | async-start | bytes 655360 | tf_op jit(solution)/shard_map/reduce_scatter | solution.py:89
  309.5 2.9 copy-start.7
  309.5 3.0 copy-start.4
  312.5 2.5 copy-start.1
  315.0 1.3 copy-start.3
  315.0 1.3 copy-start.11
  316.4 0.8 copy-start.5
  317.2 2.6 copy-start.2
  321.7 4.2 %copy-start.10 = (s32[128,2]{0,1:T(2,128)S(1)}, s32[128,2]{0,1:T(2,128)}, u32[]{:S(2)}) copy-start(s32[128,2]{0,1:T(2,128)} %param.27) | copy-start | bytes 3076
  321.7 4.4 %copy-start.14 = (f32[128,2]{0,1:T(2,128)S(1)}, f32[128,2]{0,1:T(2,128)}, u32[]{:S(2)}) copy-start(f32[128,2]{0,1:T(2,128)} %param.28) | copy-start | bytes 3076
  321.7 4.5 %copy-start.13 = (s32[256,1]{0,1:T(1,128)S(1)}, s32[256,1]{0,1:T(1,128)}, u32[]{:S(2)}) copy-start(s32[256,1]{0,1:T(1,128)} %copy-done.12) | copy-start | bytes 3076
Sparse Core Ops, SparseCore 0:
  63.6 45.3 all-gather.1
  129.6 58.8 reduce-scatter.4
  325.8 18.0 reduce-scatter.2
where the time goes:
time: 351 us; the launch traced here: 350 us
  blocking collectives  158 us (45%)
  waiting for transfers between devices  110 us (31%)
  matrix products  32.1 us (9%)
  local copies, waits for them, and re-layouts  16.1 us (5%)
  between operations  14.7 us (4%)
  other arithmetic  14 us (4%)
  starting transfers between devices  5.63 us (2%)
    reduce_scatter x1, waiting for transfers between devices, experts(): lax.psum_scatter(jnp.dot(hidden, w_down[0], preferred_element_type=jnp.fl...  58.9 us
    all_gather x1, blocking collectives, mixer(): piece_a = lax.all_gather(keys_a, 'ep', axis=0, tiled=True)  54.2 us
    all_gather x1, waiting for transfers between devices, experts(): lax.all_gather(arrived, 'tp', axis=0, tiled=True)  45.5 us
    all_to_all x1, blocking collectives, experts(): lax.all_to_all(outgoing, 'ep', split_axis=0, concat_axis=1, tiled=True)  44.2 us
    all_gather x1, blocking collectives, mixer(): piece_v = lax.all_gather(values, 'ep', axis=0, tiled=True)  31.3 us
    all_gather x1, blocking collectives, mixer(): piece_b = lax.all_gather(keys_b, 'ep', axis=0, tiled=True)  27.8 us
    dot_general x1, matrix products, experts(): jnp.dot(hidden, w_down[0], preferred_element_type=jnp.float32)  11.9 us
    dot_general x1, matrix products, hidden_rows(): gate = jnp.dot(inputs, gate_matrix, preferred_element_type=jnp.float32)  8.52 us
  transfers between devices with their start and end apart: 4, of which 3 were waited for; matrix products, arithmetic and copies ran while one was open for 8% of the time, Pallas kernels for 0%

commit v1 on v0

--- a/solution.py
+++ b/solution.py
@@ -63,7 +63,12 @@
     initial = (lowest, nothing, blank, lowest, nothing, blank)
     piece_a = lax.all_gather(keys_a, "ep", axis=0, tiled=True)
     piece_b = lax.all_gather(keys_b, "ep", axis=0, tiled=True)
-    piece_v = lax.all_gather(values, "ep", axis=0, tiled=True)
+    ring = [values]
+    for hop in range(7):
+        ring.append(lax.ppermute(ring[-1], "ep", [(dev, (dev + 1) % 8) for dev in range(8)]))
+    piece_v = jnp.roll(
+        jnp.concatenate(ring[::-1], axis=0), (lax.axis_index("ep") + 1) * ring[0].shape[0], axis=0
+    )
     count = piece_a.shape[0]
 
     def visit(state):

time: 351 us -> 279 us (0.79)
  blocking collectives: 158 us -> 97.8 us
  waiting for transfers between devices: 110 us -> 87.4 us
  local copies, waits for them, and re-layouts: 16.1 us -> 27.5 us
    reduce_scatter x1, waiting for transfers between devices: 58.9 us -> 0.01 us  [experts(): lax.psum_scatter(jnp.dot(hidden, w_down[0], preferred_element_type=jnp.fl...]
    ppermute x0 -> x7, waiting for transfers between devices: none -> 32 us  [mixer(): lax.ppermute(ring[-1], 'ep', [(dev, (dev + 1) % 8) for dev in range(8)])]
    all_gather x1 -> x0, blocking collectives: 31.3 us -> none  [mixer(): piece_v = lax.all_gather(values, 'ep', axis=0, tiled=True)]
    all_gather x1, blocking collectives: 54.2 us -> 27.1 us  [mixer(): piece_a = lax.all_gather(keys_a, 'ep', axis=0, tiled=True)]
    unnamed x22 -> x40, local copies, waits for them, and re-layouts: 1.32 us -> 11.9 us
    ppermute x0 -> x7, starting transfers between devices: none -> 3.54 us  [mixer(): lax.ppermute(ring[-1], 'ep', [(dev, (dev + 1) % 8) for dev in range(8)])]
  transfers between devices with their start and end apart: 4 -> 11, of which waited for: 3 -> 8; matrix products, arithmetic and copies ran while one was open for 8% -> 13% of each run, Pallas kernels for 0% -> 0%
where the time goes in v1:
time: 279 us; the launch traced here: 278 us
  blocking collectives  97.8 us (35%)
  waiting for transfers between devices  87.4 us (31%)
  matrix products  29.2 us (10%)
  local copies, waits for them, and re-layouts  27.5 us (10%)
  between operations  14.6 us (5%)
  other arithmetic  13.3 us (5%)
  starting transfers between devices  8.1 us (3%)
    all_gather x1, waiting for transfers between devices, experts(): lax.all_gather(arrived, 'tp', axis=0, tiled=True)  45.5 us
    all_to_all x1, blocking collectives, experts(): lax.all_to_all(outgoing, 'ep', split_axis=0, concat_axis=1, tiled=True)  44.2 us
    ppermute x7, waiting for transfers between devices, mixer(): lax.ppermute(ring[-1], 'ep', [(dev, (dev + 1) % 8) for dev in range(8)])  32 us
    all_gather x1, blocking collectives, mixer(): piece_a = lax.all_gather(keys_a, 'ep', axis=0, tiled=True)  27.1 us
    all_gather x1, blocking collectives, mixer(): piece_b = lax.all_gather(keys_b, 'ep', axis=0, tiled=True)  26.5 us
    dot_general x1, matrix products, experts(): jnp.dot(hidden, w_down[0], preferred_element_type=jnp.float32)  11.9 us
    unnamed x40, local copies, waits for them, and re-layouts  11.9 us
    reduce_scatter x1, waiting for transfers between devices, mixer(): lax.psum_scatter(jnp.einsum('gjrv,gjvd->rd', heads_out, weights_out, pref...  8.68 us
  transfers between devices with their start and end apart: 11, of which 8 were waited for; matrix products, arithmetic and copies ran while one was open for 13% of the time, Pallas kernels for 0%

profile of v1, /device:TPU:0, one launch (start us, length us, event | category | flops | bytes accessed | tf_op | source)
XLA Modules:
  0.0 278.0 jit_solution(17752843123987090205)
XLA Ops:
  7.2 0.9 copy.55
  8.2 0.1 eq.29
  8.3 0.1 reshape.176
  8.4 0.7 broadcast_multiply_fusion
  9.1 0.6 reduce-window.6
  9.7 0.2 slice_reduce_fusion
  10.1 0.1 copy.59
  10.2 0.1 mul.127
  10.3 1.4 scatter_custom_fusion
  12.0 1.2 fusion.25
  13.2 1.2 fusion.27
  14.4 3.1 %gather_fusion = bf16[384,2048]{1,0:T(8,128)(2,1)} fusion(bf16[128,2048]{1,0:T(8,128)(2,1)S(1)} %fusion.27, s32[1024]{0:T(1024)S(1)} %pad_clamp_fusion.1), kind=kCustom, calls=%fused_computation | custom fusion | bytes 3147264 | tf_op jit(solution)/shard_map/jit(_take)/gather | solution.py:29
  17.6 1.7 select_select_fusion
  19.2 44.2 %all_to_all.14 = bf16[8,48,2048]{2,1,0:T(8,128)(2,1)} all-to-all(bf16[8,48,2048]{2,1,0:T(8,128)(2,1)S(1)} %select_select_fusion), channel_id=1, replica_groups=mesh['ep'=8,'tp'=4] {'ep'}, dimensions={0} | all-to-all | bytes 3145728 | tf_op jit(solution)/shard_map/all_to_all | solution.py:122
  63.5 45.5 %all-gather.2.cloned.1.call-done = bf16[1536,2048]{1,0:T(8,128)(2,1)} async-done(((bf16[384,2048]{1,0:T(8,128)(2,1)}), bf16[1536,2048]{1,0:T(8,128)(2,1)}) %all-gather.2.cloned.1.call-update) | async-done | bytes 6291472 | tf_op jit(solution)/shard_map/all_gather | solution.py:125
  109.0 8.5 %convolution_minimum_fusion = f32[1536,512]{1,0:T(8,128)} fusion(bf16[1536,2048]{1,0:T(8,128)(2,1)} %all-gather.2.cloned.1.call-done, bf16[1,2048,512]{2,1,0:T(8,128)(2,1)} %param.29), kind=kOutput, calls=%fused_computation.29 | convolution fusion | flops 3222011904 | bytes 11534336 | tf_op jit(solution)/shard_map/dot_general | solution.py:22
  117.5 11.9 %convolution_convert_fusion = bf16[1536,2048]{1,0:T(8,128)(2,1)} fusion(bf16[1,512,2048]{2,1,0:T(8,128)(2,1)S(1)} %copy-done, bf16[1536,2048]{1,0:T(8,128)(2,1)} %all-gather.2.cloned.1.call-done, f32[1536,512]{1,0:T(8,128)} %convolution_minimum_fusion, bf16[1,2048,512]{2,1,0:T(8,128)(2,1)} %param.30), kind=kOutput, calls=%fused_computation.27 | convolution fusion | flops 6452674560 | bytes 19922944 | tf_op jit(solution)/shard_map/dot_general | solution.py:127
  129.5 0.8 copy-done.3
  130.4 1.5 collective-permute-start
  131.9 5.5 %collective-permute-done = bf16[128,256]{0,1:T(8,128)(2,1)S(1)} collective-permute-done((bf16[128,256]{0,1:T(8,128)(2,1)S(1)}, bf16[128,256]{0,1:T(8,128)(2,1)S(1)}, u32[]{:S(2)}, u32[]{:S(2)}) %collective-permute-start) | collective-permute-done | bytes 65568 | tf_op jit(solution)/shard_map/ppermute | solution.py:68
  137.4 7.0 %collective-permute-done.1 = bf16[128,256]{0,1:T(8,128)(2,1)S(1)} collective-permute-done((bf16[128,256]{0,1:T(8,128)(2,1)S(1)}, bf16[128,256]{0,1:T(8,128)(2,1)S(1)}, u32[]{:S(2)}, u32[]{:S(2)}) %collective-permute-start.1) | collective-permute-done | bytes 65568 | tf_op jit(solution)/shard_map/ppermute | solution.py:68
  144.4 7.0 %collective-permute-done.2 = bf16[128,256]{0,1:T(8,128)(2,1)S(1)} collective-permute-done((bf16[128,256]{0,1:T(8,128)(2,1)S(1)}, bf16[128,256]{0,1:T(8,128)(2,1)S(1)}, u32[]{:S(2)}, u32[]{:S(2)}) %collective-permute-start.2) | collective-permute-done | bytes 65568 | tf_op jit(solution)/shard_map/ppermute | solution.py:68
  151.5 0.1 copy.48
  151.6 6.7 %collective-permute-done.3 = bf16[128,256]{0,1:T(8,128)(2,1)S(1)} collective-permute-done((bf16[128,256]{0,1:T(8,128)(2,1)S(1)}, bf16[128,256]{0,1:T(8,128)(2,1)S(1)}, u32[]{:S(2)}, u32[]{:S(2)}) %collective-permute-start.3) | collective-permute-done | bytes 65568 | tf_op jit(solution)/shard_map/ppermute | solution.py:68
  158.3 0.6 slice.9
  159.7 5.8 %collective-permute-done.4 = bf16[128,256]{0,1:T(8,128)(2,1)S(1)} collective-permute-done((bf16[128,256]{0,1:T(8,128)(2,1)S(1)}, bf16[128,256]{0,1:T(8,128)(2,1)S(1)}, u32[]{:S(2)}, u32[]{:S(2)}) %collective-permute-start.4) | collective-permute-done | bytes 65568 | tf_op jit(solution)/shard_map/ppermute | solution.py:68
  165.5 26.5 %all_gather.10 = bf16[1024,128]{0,1:T(8,128)(2,1)S(1)} all-gather(bf16[128,128]{0,1:T(8,128)(2,1)S(1)} %copy.52), channel_id=1, replica_groups=mesh['ep'=8,'tp'=4] {'ep'}, dimensions={0}, use_global_device_ids=true | all-gather | bytes 294912 | tf_op jit(solution)/shard_map/all_gather | solution.py:65
  192.0 2.0 collective-permute-start.6
  194.0 27.1 %all_gather.9 = bf16[1024,128]{0,1:T(8,128)(2,1)S(1)} all-gather(bf16[128,128]{0,1:T(8,128)(2,1)S(1)} %copy.48), channel_id=1, replica_groups=mesh['ep'=8,'tp'=4] {'ep'}, dimensions={0}, use_global_device_ids=true | all-gather | bytes 294912 | tf_op jit(solution)/shard_map/all_gather | solution.py:64
  221.0 0.7 constant_dynamic-update-slice_fusion.15
  221.7 0.7 constant_dynamic-update-slice_fusion.14
  222.3 0.6 constant_dynamic-update-slice_fusion.13
  223.0 0.6 constant_dynamic-update-slice_fusion.12
  223.6 4.4 %all-to-all-start.1 = ((bf16[8,48,2048]{2,1,0:T(8,128)(2,1)}), bf16[8,48,2048]{2,1,0:T(8,128)(2,1)}, u32[]{:S(2)}, u32[]{:S(2)}) async-start(bf16[8,48,2048]{2,1,0:T(8,128)(2,1)} %bitcast.83), calls=%async_computation.3 | async-start | bytes 3145728 | tf_op jit(solution)/shard_map/all_to_all | solution.py:132
  228.1 0.6 constant_dynamic-update-slice_fusion.11
  228.8 0.7 constant_dynamic-update-slice_fusion.10
  229.4 0.6 constant_dynamic-update-slice_fusion.9
  230.1 0.7 constant_dynamic-update-slice_fusion.8
  230.7 0.7 constant_dynamic-update-slice_fusion.7
  231.4 0.6 constant_dynamic-update-slice_fusion.6
  232.0 0.6 constant_dynamic-update-slice_fusion.5
  232.7 0.6 constant_dynamic-update-slice_fusion.4
  233.3 0.6 constant_dynamic-update-slice_fusion.3
  233.9 0.6 constant_dynamic-update-slice_fusion.2
  234.6 0.6 constant_dynamic-update-slice_fusion.1
  235.2 0.7 constant_dynamic-update-slice_fusion
  235.9 10.1 %conditional.1 = (f32[2,2,128]{2,1,0:T(2,128)S(1)}, f32[2,2,128,128]{3,2,1,0:T(8,128)S(1)}, f32[2,2,128]{2,1,0:T(2,128)S(1)}, f32[2,2,128,128]{3,2,1,0:T(8,128)S(1)}) conditional(s32[]{:T(128)} %bitcast, () %tuple.27, (s32[128]{0:T(128)S(1)}, bf16[1024,128]{0,1:T(8,128)(2,1)S(1)}, bf16[128,256]{1,0:T(8,128)(2,1)S(1)}, s32[]{:T(128)}, s32[]{:T(128)}, ...), branch_computations={%region_0.1_spmd, %region_1.6_spmd.clone} | conditional | flops 416414720 | bytes 29385456 | solution.py:86
  235.9 2.1 constant_dynamic-slice_fusion
  238.1 0.1 copy.53
  238.2 1.8 fusion.40
  240.2 2.3 fusion.1
  242.5 0.9 fusion.6
  243.4 0.7 copy-done.1
  244.1 0.8 fusion.8
  245.0 1.0 fusion.5
  246.0 0.3 multiply_reduce_fusion.1
  246.4 2.9 %fusion.21 = bf16[128,2048]{1,0:T(8,128)(2,1)} fusion(bf16[2,2,128,2048]{3,2,1,0:T(8,128)(2,1)} %bitcast.82, f32[2,2,128,128]{3,2,1,0:T(8,128)S(1)} %get-tuple-element.196, f32[128]{0:T(128)S(1)} %copy-done.10, f32[2,2,128]{2,1,0:T(2,128)S(1)} %add_rsqrt_fusion), kind=kOutput, calls=%fused_computation.34 | convolution fusion | flops 268894208 | bytes 2886144 | tf_op jit(solution)/shard_map/gjrv,gjvd->rd/dot_general | solution.py:95
  249.3 0.1 sub.56
  249.5 0.1 copy.58
  249.8 1.2 all-to-all-done.1
  251.0 4.0 %gather_fusion.1 = bf16[256,2048]{1,0:T(8,128)(2,1)S(1)} fusion(bf16[384,2048]{1,0:T(8,128)(2,1)} %bitcast.14, s32[1024]{0:T(1024)S(1)} %pad_clamp_fusion), kind=kCustom, calls=%fused_computation.1 | custom fusion | bytes 2098176 | tf_op jit(solution)/shard_map/jit(_take)/gather | solution.py:135
  255.0 1.5 gather.15
  256.5 6.3 %multiply_reduce_fusion = bf16[128,2048]{1,0:T(8,128)(2,1)} fusion(bf16[128,2,2048]{2,1,0:T(2,128)(2,1)} %gather.15, pred[128,2]{1,0:T(8,128)(4,1)S(1)} %copy.58, f32[128,2]{1,0:T(8,128)S(1)} %copy.60), kind=kLoop, calls=%fused_computation.38 | loop fusion | flops 1835008 | bytes 1574144 | tf_op jit(solution)/shard_map/reduce_sum | solution.py:136
  262.8 8.7 %reduce-scatter.3.cloned.1.call-done = bf16[32,2048]{1,0:T(8,128)(2,1)} async-done(((bf16[128,2048]{1,0:T(8,128)(2,1)}), bf16[32,2048]{1,0:T(8,128)(2,1)}) %reduce-scatter.3.cloned.1.call-update) | async-done | bytes 131088 | tf_op jit(solution)/shard_map/reduce_scatter | solution.py:94
  (61 shorter events, 1.3 us)
Async XLA Ops:
  7.2 110.4 %copy-start = (bf16[1,512,2048]{2,1,0:T(8,128)(2,1)S(1)}, bf16[1,512,2048]{2,1,0:T(8,128)(2,1)}, u32[]{:S(2)}) copy-start(bf16[1,512,2048]{2,1,0:T(8,128)(2,1)} %param.31) | copy-start | bytes 6291460
  7.2 101.8 %all-gather.2.cloned.1.call-start = ((), (), s32[]{:S(2)}) async-start(), calls=%async_computation.5 | async-start | bytes 7864320 | tf_op jit(solution)/shard_map/all_gather | solution.py:125
  63.5 160.2 %reduce-scatter.5.cloned.1.call-start = ((), (), s32[]{:S(2)}) async-start(), calls=%async_computation.6 | async-start | bytes 7864320 | tf_op jit(solution)/shard_map/reduce_scatter | solution.py:126
  129.5 0.8 copy-start.3
  129.5 21.9 %copy-start.6 = (bf16[128,128]{1,0:T(8,128)(2,1)S(1)}, bf16[128,128]{1,0:T(8,128)(2,1)}, u32[]{:S(2)}) copy-start(bf16[128,128]{1,0:T(8,128)(2,1)} %param.20) | copy-start | bytes 98308
  129.5 22.0 %copy-start.7 = (bf16[128,128]{1,0:T(8,128)(2,1)S(1)}, bf16[128,128]{1,0:T(8,128)(2,1)}, u32[]{:S(2)}) copy-start(bf16[128,128]{1,0:T(8,128)(2,1)} %param.19) | copy-start | bytes 98308
  129.5 30.1 %copy-start.11 = (f32[4]{0:T(128)S(1)}, f32[4]{0:T(128)}, u32[]{:S(2)}) copy-start(f32[4]{0:T(128)} %param.22) | copy-start | bytes 52
  130.4 7.0 %collective-permute-start = (bf16[128,256]{0,1:T(8,128)(2,1)S(1)}, bf16[128,256]{0,1:T(8,128)(2,1)S(1)}, u32[]{:S(2)}, u32[]{:S(2)}) collective-permute-start(bf16[128,256]{0,1:T(8,128)(2,1)S(1)} %copy.49), channel_id=1, source_target_pairs={{0,4},{4,8},{8,12},{12,16},{16,20},{20,24},{24,28},{28,0},{1,5},{5... | collective-permute-start | bytes 196616 | tf_op jit(solution)/shard_map/ppermute | solution.py:68
  137.4 7.0 %collective-permute-start.1 = (bf16[128,256]{0,1:T(8,128)(2,1)S(1)}, bf16[128,256]{0,1:T(8,128)(2,1)S(1)}, u32[]{:S(2)}, u32[]{:S(2)}) collective-permute-start(bf16[128,256]{0,1:T(8,128)(2,1)S(1)} %collective-permute-done), channel_id=1, source_target_pairs={{0,4},{4,8},{8,12},{12,16},{16,20},{20,24},{24,28},{28,0},{1,5},{5... | collective-permute-start | bytes 196616 | tf_op jit(solution)/shard_map/ppermute | solution.py:68
  144.4 7.0 %collective-permute-start.2 = (bf16[128,256]{0,1:T(8,128)(2,1)S(1)}, bf16[128,256]{0,1:T(8,128)(2,1)S(1)}, u32[]{:S(2)}, u32[]{:S(2)}) collective-permute-start(bf16[128,256]{0,1:T(8,128)(2,1)S(1)} %collective-permute-done.1), channel_id=1, source_target_pairs={{0,4},{4,8},{8,12},{12,16},{16,20},{20,24},{24,28},{28,0},{1,5},{5... | collective-permute-start | bytes 196616 | tf_op jit(solution)/shard_map/ppermute | solution.py:68
  151.4 7.0 %collective-permute-start.3 = (bf16[128,256]{0,1:T(8,128)(2,1)S(1)}, bf16[128,256]{0,1:T(8,128)(2,1)S(1)}, u32[]{:S(2)}, u32[]{:S(2)}) collective-permute-start(bf16[128,256]{0,1:T(8,128)(2,1)S(1)} %collective-permute-done.2), channel_id=1, source_target_pairs={{0,4},{4,8},{8,12},{12,16},{16,20},{20,24},{24,28},{28,0},{1,5},{5... | collective-permute-start | bytes 196616 | tf_op jit(solution)/shard_map/ppermute | solution.py:68
  158.3 7.2 %collective-permute-start.4 = (bf16[128,256]{0,1:T(8,128)(2,1)S(1)}, bf16[128,256]{0,1:T(8,128)(2,1)S(1)}, u32[]{:S(2)}, u32[]{:S(2)}) collective-permute-start(bf16[128,256]{0,1:T(8,128)(2,1)S(1)} %collective-permute-done.3), channel_id=1, source_target_pairs={{0,4},{4,8},{8,12},{12,16},{16,20},{20,24},{24,28},{28,0},{1,5},{5... | collective-permute-start | bytes 196616 | tf_op jit(solution)/shard_map/ppermute | solution.py:68
  165.5 26.5 %collective-permute-start.5 = (bf16[128,256]{0,1:T(8,128)(2,1)S(1)}, bf16[128,256]{0,1:T(8,128)(2,1)S(1)}, u32[]{:S(2)}, u32[]{:S(2)}) collective-permute-start(bf16[128,256]{0,1:T(8,128)(2,1)S(1)} %collective-permute-done.4), channel_id=1, source_target_pairs={{0,4},{4,8},{8,12},{12,16},{16,20},{20,24},{24,28},{28,0},{1,5},{5... | collective-permute-start | bytes 196616 | tf_op jit(solution)/shard_map/ppermute | solution.py:68
  192.0 29.1 %collective-permute-start.6 = (bf16[128,256]{0,1:T(8,128)(2,1)S(1)}, bf16[128,256]{0,1:T(8,128)(2,1)S(1)}, u32[]{:S(2)}, u32[]{:S(2)}) collective-permute-start(bf16[128,256]{0,1:T(8,128)(2,1)S(1)} %collective-permute-done.5), channel_id=1, source_target_pairs={{0,4},{4,8},{8,12},{12,16},{16,20},{20,24},{24,28},{28,0},{1,5},{5... | collective-permute-start | bytes 196616 | tf_op jit(solution)/shard_map/ppermute | solution.py:68
  223.6 12.2 %copy-start.4 = (bf16[128,256]{1,0:T(8,128)(2,1)S(1)}, bf16[128,256]{1,0:T(8,128)(2,1)}, u32[]{:S(2)}) copy-start(bf16[128,256]{1,0:T(8,128)(2,1)} %param.17) | copy-start | bytes 196612
  223.6 12.2 %copy-start.5 = (bf16[128,256]{1,0:T(8,128)(2,1)S(1)}, bf16[128,256]{1,0:T(8,128)(2,1)}, u32[]{:S(2)}) copy-start(bf16[128,256]{1,0:T(8,128)(2,1)} %param.18) | copy-start | bytes 196612
  223.6 27.4 %all-to-all-start.1 = ((bf16[8,48,2048]{2,1,0:T(8,128)(2,1)}), bf16[8,48,2048]{2,1,0:T(8,128)(2,1)}, u32[]{:S(2)}, u32[]{:S(2)}) async-start(bf16[8,48,2048]{2,1,0:T(8,128)(2,1)} %bitcast.83), calls=%async_computation.3 | async-start | bytes 3145728 | tf_op jit(solution)/shard_map/all_to_all | solution.py:132
  228.1 43.4 %reduce-scatter.3.cloned.1.call-start = ((), (), s32[]{:S(2)}) async-start(), calls=%async_computation.4 | async-start | bytes 655360 | tf_op jit(solution)/shard_map/reduce_scatter | solution.py:94
  235.9 10.5 %copy-start.10 = (f32[128]{0:T(128)S(1)}, f32[128]{0:T(128)}, u32[]{:S(2)}) copy-start(f32[128]{0:T(128)} %param.23) | copy-start | bytes 1540
  240.2 2.3 copy-start.2
  242.5 1.6 copy-start.1
  246.0 3.5 %copy-start.8 = (s32[128,2]{0,1:T(2,128)S(1)}, s32[128,2]{0,1:T(2,128)}, u32[]{:S(2)}) copy-start(s32[128,2]{0,1:T(2,128)} %param.27) | copy-start | bytes 3076
  246.0 3.7 %copy-start.9 = (f32[128,2]{0,1:T(2,128)S(1)}, f32[128,2]{0,1:T(2,128)}, u32[]{:S(2)}) copy-start(f32[128,2]{0,1:T(2,128)} %param.28) | copy-start | bytes 3076
Sparse Core Ops, SparseCore 0:
  63.6 45.3 all-gather.1
  129.6 58.8 reduce-scatter.4
  249.4 22.0 reduce-scatter.2
